TPU v7x, 32 devices: a whole 2x2x4 slice. The times are simulated.
32 devices in a mesh: grp: 2 (over y), sp: 4 (over z), tp: 4 (over x, core).
Axes of the slice: x: 2, y: 2, z: 4, core: 2. Of those that a mesh axis runs over, the one named last changes fastest.
Arguments:
- layer_input: bfloat16 [4, 2048, 2048], P('grp', 'sp'), parts along dimension 0, may hold values from -6 to 6
- key_weight: bfloat16 [2048, 1024], P(None, 'tp'), may hold values from -0.125 to 0.125
- value_weight: bfloat16 [2048, 1024], P(None, 'tp'), may hold values from -0.125 to 0.125
- beta_weight: bfloat16 [2048, 8], replicated, may hold values from -0.125 to 0.125
- beta_shift: float32 [8], replicated
- decay_weight: bfloat16 [2048, 8], replicated, may hold values from -0.125 to 0.125
- decay_rate: float32 [8], replicated, may hold values from 0 to 0.05
- decay_extra: float32 [4, 2048, 8], P('grp', 'sp', 'tp'), parts along dimension 0, may hold values from -1.5 to 0
- query_new: bfloat16 [4, 1024], P('grp', 'tp'), parts along dimension 0, may hold values from -6 to 6
- gate_new: bfloat16 [4, 1024], P('grp', 'tp'), parts along dimension 0, may hold values from -6 to 6
- norm_gain: float32 [128], replicated, may hold values from 0.1 to 1.9
- out_weight: bfloat16 [8, 128, 2048], P('tp', 'sp'), may hold values from -0.1875 to 0.1875
Outputs:
- state_cache: bfloat16 [4, 8, 128, 128], P('grp', 'tp', None, 'sp'), parts along dimension 0
- read_out: float32 [4, 2048], P('grp', ('sp', 'tp')), parts along dimension 0
There are 2 independent parts, one for each index of `grp`. A program takes and returns all parts, laid end to end along the dimension named above; an argument that names none is the same for every part. Nothing has to cross between parts.
All inputs are finite; a program needn't handle non-finite values.
Results may differ from a plain program's by a relative error of at most 0.013.
Values sent between devices are 32-bit elements; how exact they have to be, the bound alone decides.
A program may use at most 64 MiB of HBM per device.

v0:
```python
import jax
import jax.numpy as jnp
from jax import lax
from jax.sharding import PartitionSpec as P

DK = 128
BLK = 64


epsilon = 1e-06
highest = lax.Precision.HIGHEST


def entering(shard, axis, combine, identity):
    size, here = (lax.axis_size(axis), lax.axis_index(axis))
    everything = lax.all_gather(shard, axis)
    start = jnp.broadcast_to(jnp.asarray(identity, shard.dtype), shard.shape)

    def turn(k, before):
        at = size - 1 - k
        reached = at > here
        new = combine(before, everything[at])
        return jnp.where(reached, new, before)

    return lax.fori_loop(0, size, turn, start)


def local_map(key_rows, value_rows, beta, log_decay, span):
    seq_here, length, heads_here, head_size = key_rows.shape
    block_count = length // span
    unit_keys = key_rows * lax.rsqrt(jnp.sum(key_rows * key_rows, axis=-1, keepdims=True) + epsilon)

    def blocked(tensor):
        moved_axes = jnp.moveaxis(tensor, 2, 1)
        return moved_axes.reshape((seq_here, heads_here, block_count, span) + tensor.shape[3:])

    key_blocks = blocked(unit_keys)
    value_blocks = blocked(value_rows)
    beta_blocks = blocked(beta)
    cumulative = jnp.cumsum(blocked(log_decay), axis=-1)
    places = jnp.arange(span)
    strict = places[:, None] > places[None, :]
    weighted = key_blocks * beta_blocks[..., None]
    key_products = jnp.einsum("shnid,shnjd->shnij", weighted, key_blocks, precision=highest)
    spread = cumulative[..., :, None] - cumulative[..., None, :]
    lower_part = jnp.where(strict, key_products * jnp.exp(jnp.where(strict, spread, 0.0)), 0.0)
    system = jnp.eye(span, dtype=jnp.float32) + lower_part
    right_side = jnp.concatenate(
        [value_blocks * beta_blocks[..., None], weighted * jnp.exp(cumulative)[..., None]], axis=-1
    )
    solved = jax.scipy.linalg.solve_triangular(system, right_side, lower=True)
    value_part = solved[..., :head_size]
    key_part = solved[..., head_size:]
    carried_keys = key_blocks * jnp.exp(cumulative[..., -1:] - cumulative)[..., None]
    block_decay = jnp.exp(cumulative[..., -1])
    sequence_in = tuple(
        (jnp.moveaxis(tensor, 2, 0) for tensor in (value_part, key_part, carried_keys, block_decay))
    )
    zero_half = jnp.zeros((seq_here, heads_here, head_size, head_size), jnp.float32)

    def advance(carry_map, inputs):
        value_now, key_now, carried_now, decay_now = inputs
        mixed = jnp.einsum("shck,shkx->shcx", key_now, carry_map, precision=highest)
        written = jnp.einsum("shck,shcv->shkv", carried_now, value_now, precision=highest)
        carry_map = (
            carry_map * decay_now[..., None, None]
            - jnp.einsum("shck,shcx->shkx", carried_now, mixed, precision=highest)
            + jnp.concatenate([zero_half, written], axis=-1)
        )
        return (carry_map, None)

    identity = jnp.broadcast_to(jnp.eye(head_size, dtype=jnp.float32), zero_half.shape)
    initial = jnp.concatenate([identity, zero_half], axis=-1)
    whole_map, unused = lax.scan(advance, initial, sequence_in)
    return (whole_map[..., :head_size], whole_map[..., head_size:])


def compose(earlier, later):
    return jnp.einsum("shij,shjk->shik", earlier, later, precision=highest)


def per_device(
    layer_input,
    key_weight,
    value_weight,
    beta_weight,
    beta_shift,
    decay_weight,
    decay_rate,
    decay_extra,
    query_new,
    gate_new,
    norm_gain,
    out_weight,
):
    head_size = DK
    heads_here = key_weight.shape[1] // head_size
    seq_here, places_here, unused_width = layer_input.shape
    first_head = lax.axis_index("tp") * heads_here
    beta_cols = lax.dynamic_slice_in_dim(beta_weight, first_head, heads_here, 1)
    decay_cols = lax.dynamic_slice_in_dim(decay_weight, first_head, heads_here, 1)
    head_rates = lax.dynamic_slice_in_dim(decay_rate, first_head, heads_here, 0)
    head_shift = lax.dynamic_slice_in_dim(beta_shift, first_head, heads_here, 0)
    key_rows = jnp.dot(layer_input, key_weight, preferred_element_type=jnp.float32).astype(
        jnp.bfloat16
    )
    value_rows = jnp.dot(layer_input, value_weight, preferred_element_type=jnp.float32).astype(
        jnp.bfloat16
    )
    beta_raw = jnp.dot(layer_input, beta_cols, preferred_element_type=jnp.float32).astype(
        jnp.bfloat16
    )
    decay_raw = jnp.dot(layer_input, decay_cols, preferred_element_type=jnp.float32).astype(
        jnp.bfloat16
    )
    beta = jax.nn.sigmoid(beta_raw.astype(jnp.float32) + head_shift)
    log_decay = -head_rates * jax.nn.softplus(decay_raw.astype(jnp.float32)) + decay_extra
    linear_part, offset_part = local_map(
        key_rows.reshape(seq_here, places_here, heads_here, head_size).astype(jnp.float32),
        value_rows.reshape(seq_here, places_here, heads_here, head_size).astype(jnp.float32),
        beta,
        log_decay,
        BLK,
    )
    eye_maps = jnp.broadcast_to(jnp.eye(head_size, dtype=jnp.float32), linear_part.shape)
    column_count = head_size // lax.axis_size("sp")
    first_column = lax.axis_index("sp") * column_count
    after_maps = entering(linear_part, "sp", compose, eye_maps)
    own_term = compose(after_maps, offset_part)
    own_state = lax.psum_scatter(own_term, "sp", scatter_dimension=3, tiled=True)
    state_cache = own_state.astype(jnp.bfloat16)
    query = query_new.reshape(seq_here, heads_here, head_size).astype(jnp.float32)
    query = (
        query
        * lax.rsqrt(jnp.sum(query * query, axis=-1, keepdims=True) + epsilon)
        * head_size ** (-0.5)
    )
    readout = jnp.einsum("shkv,shk->shv", own_state, query, precision=highest)
    squares = lax.psum(jnp.sum(readout * readout, axis=-1), "sp")
    scaled = readout * lax.rsqrt(squares[..., None] / head_size + epsilon)
    gate_values = lax.dynamic_slice_in_dim(
        gate_new.reshape(seq_here, heads_here, head_size), first_column, column_count, 2
    ).astype(jnp.float32)
    gain_here = lax.dynamic_slice_in_dim(norm_gain, first_column, column_count, 0)
    normed = (scaled * gain_here * jax.nn.silu(gate_values)).astype(jnp.bfloat16)
    partial_value = jnp.einsum(
        "shc,hcd->sd", normed, out_weight, preferred_element_type=jnp.float32
    )
    summed = lax.psum_scatter(partial_value, ("sp", "tp"), scatter_dimension=1, tiled=True)
    return (state_cache, summed)


def solution(mesh):
    return jax.shard_map(
        per_device,
        mesh=mesh,
        in_specs=(
            P("grp", "sp", None),
            P(None, "tp"),
            P(None, "tp"),
            P(),
            P(),
            P(),
            P(),
            P("grp", "sp", "tp"),
            P("grp", "tp"),
            P("grp", "tp"),
            P(),
            P("tp", "sp", None),
        ),
        out_specs=(P("grp", "tp", None, "sp"), P("grp", ("sp", "tp"))),
        check_vma=False,
    )
```

profile of v0, /device:TPU:0, one launch (start us, length us, event | category | flops | bytes accessed | tf_op | source)
XLA Modules:
  0.0 356.1 jit_solution(7586617026521847361)
XLA Ops:
  8.1 3.4 fusion.61
  12.8 3.4 fusion.46
  16.3 3.5 fusion.49
  20.3 3.8 %convolution_convert_fusion = bf16[2,512,256]{1,2,0:T(8,128)(2,1)S(1)} fusion(bf16[2,512,2048]{2,1,0:T(8,128)(2,1)} %param.16, bf16[2048,256]{1,0:T(8,128)(2,1)} %param.18), kind=kOutput, calls=%fused_computation.37 | convolution fusion | flops 1074003968 | bytes 5767168 | tf_op jit(solution)/shard_map/dot_general | solution.py:107
  25.6 1.9 fusion.37
  27.5 158.0 %custom-call.4 = f32[2,2,8,1,64,64]{4,5,3,2,1,0:T(8,128)} custom-call(f32[2,2,8,1,64,64]{5,4,3,2,1,0:T(8,128)S(1)} %fusion.37), custom_call_target="InvertDiagBlocksLowerTriangular" | custom-call | tf_op jit(solution)/shard_map/jit(_solve_triangular)/vmap(vmap(vmap()))/triangular_solve | solution.py:51
  185.5 2.1 multiply_multiply_fusion
  187.6 2.0 fusion.19
  189.6 1.6 slice_bitcast_fusion
  191.5 29.2 %while.25 = (s32[]{:T(128)}, f32[2,2,128,256]{3,2,1,0:T(8,128)S(1)}, f32[8,2,2]{2,1,0:T(2,128)S(1)}, f32[8,2,2,64,128]{4,3,0,2,1:T(8,128)S(1)}, f32[8,2,2,64,128...) while((s32[]{:T(128)}, f32[2,2,128,256]{3,2,1,0:T(8,128)S(1)}, f32[8,2,2]{2,1,0:T(2,128)S(1)}, ...), condition=%wide.region_3.4_spmd, body=%wide.region_2.3_spmd.sunk | while | flops 252051456 | bytes 3148405 | solution.py:74
  191.5 1.5 fusion.118
  195.2 1.5 fusion.118
  198.8 1.5 fusion.118
  202.5 1.5 fusion.118
  221.8 30.5 %all-gather.3.cloned.1.call-done = f32[8,2,128,128]{3,2,1,0:T(8,128)} async-done(((f32[2,2,128,128]{3,2,1,0:T(8,128)}), f32[8,2,128,128]{3,2,1,0:T(8,128)}) %all-gather.3.cloned.1.call-update) | async-done | bytes 1048592 | tf_op jit(solution)/shard_map/all_gather | solution.py:16
  252.3 6.5 %while.26 = (s32[]{:T(128)}, f32[2,2,128,128]{2,3,1,0:T(8,128)S(1)}, s32[]{:T(128)}, f32[4,2,2,128,128]{4,3,2,1,0:T(8,128)}, s32[]{:T(128)}, /*index=5*/s32[]{:T(128)}, s32[]{:T(128)}, s32[]{:T(128)}) while((s32[]{:T(128)}, f32[2,2,128,128]{2,3,1,0:T(8,128)S(1)}, s32[]{:T(128)}, f32[4,2,2,128,128]{4,3,2,1,0:T(8,128)}, s32[]{:T(128)}, ...), condition=%wide.region_5.6_spmd, body=%wide.region_4.5_spmd.sunk | while | flops 100728840 | bytes 1573009 | solution.py:25
  252.4 1.6 fusion.123
  254.0 1.6 fusion.123
  255.6 1.6 fusion.123
  257.3 1.6 fusion.123
  260.1 19.3 %reduce-scatter.5.cloned.1.call-done = f32[2,2,128,32]{2,3,1,0:T(8,128)} async-done(((f32[2,2,128,128]{2,3,1,0:T(8,128)}), f32[2,2,128,32]{2,3,1,0:T(8,128)}) %reduce-scatter.5.cloned.1.call-update) | async-done | bytes 65552 | tf_op jit(solution)/shard_map/reduce_scatter | solution.py:130
  280.8 8.7 %psum.7 = f32[2,2]{1,0:T(2,128)S(1)} all-reduce(f32[2,2]{1,0:T(2,128)S(1)} %copy.76), channel_id=1, replica_groups=mesh['grp'=2,'sp'=4,'tp'=4] {'sp'}, use_global_device_ids=true, to_apply=%region_9.10 | all-reduce | flops 4 | bytes 32 | tf_op jit(solution)/shard_map/psum | solution.py:139
  289.6 1.6 convolution_bitcast_fusion.1
  292.7 55.5 %reduce-scatter.7.cloned.1.call-done = f32[128,2]{1,0:T(8,128)} async-done(((f32[2048,2]{1,0:T(8,128)}), f32[128,2]{1,0:T(8,128)}) %reduce-scatter.7.cloned.1.call-update) | async-done | bytes 1040
  (88 shorter events, 34.0 us)
Async XLA Ops:
  7.2 9.1 %copy-start = (bf16[2048,256]{1,0:T(8,128)(2,1)S(1)}, bf16[2048,256]{1,0:T(8,128)(2,1)}, u32[]{:S(2)}) copy-start(bf16[2048,256]{1,0:T(8,128)(2,1)} %param.17) | copy-start | bytes 3145732
  7.2 5.5 %copy-start.5 = (f32[8]{0:T(128)S(1)}, f32[8]{0:T(128)}, u32[]{:S(2)}) copy-start(f32[8]{0:T(128)} %param.20) | copy-start | bytes 100
  7.2 245.1 %all-gather.3.cloned.1.call-start = ((), (), s32[]{:S(2)}) async-start(), calls=%async_computation.3 | async-start | bytes 1310720 | tf_op jit(solution)/shard_map/all_gather | solution.py:16
  185.4 2.1 copy-start.1
  191.5 30.2 %copy-start.3 = (bf16[2,256]{1,0:T(2,128)(2,1)S(1)}, bf16[2,256]{1,0:T(2,128)(2,1)}, u32[]{:S(2)}) copy-start(bf16[2,256]{1,0:T(2,128)(2,1)} %param.24) | copy-start | bytes 3076
  221.5 58.0 %reduce-scatter.5.cloned.1.call-start = ((), (), s32[]{:S(2)}) async-start(), calls=%async_computation.2 | async-start | bytes 327680 | tf_op jit(solution)/shard_map/reduce_scatter | solution.py:130
  221.7 59.0 %copy-start.6 = (f32[128]{0:T(128)S(1)}, f32[128]{0:T(128)}, u32[]{:S(2)}) copy-start(f32[128]{0:T(128)} %param.26) | copy-start | bytes 1540
  221.7 67.9 %copy-start.2 = (bf16[2,32,2048]{2,1,0:T(8,128)(2,1)S(1)}, bf16[2,32,2048]{2,1,0:T(8,128)(2,1)}, u32[]{:S(2)}) copy-start(bf16[2,32,2048]{2,1,0:T(8,128)(2,1)} %param.27) | copy-start | bytes 786436
  221.7 67.9 %copy-start.4 = (bf16[2,256]{1,0:T(2,128)(2,1)S(1)}, bf16[2,256]{1,0:T(2,128)(2,1)}, u32[]{:S(2)}) copy-start(bf16[2,256]{1,0:T(2,128)(2,1)} %param.25) | copy-start | bytes 3076
  259.9 88.2 %reduce-scatter.7.cloned.1.call-start = ((), (), s32[]{:S(2)}) async-start(), calls=%async_computation.4 | async-start | bytes 1114112
Sparse Core Ops, SparseCore 0:
  221.6 30.6 all-gather.2
  260.1 19.3 reduce-scatter.4
  291.3 56.7 reduce-scatter.6
where the time goes:
time: 357 us; the launch traced here: 356 us
  other arithmetic  164 us (46%)
  waiting for transfers between devices  105 us (29%)
  matrix products  56.7 us (16%)
  between operations  14 us (4%)
  blocking collectives  8.73 us (2%)
  local copies, waits for them, and re-layouts  6.85 us (2%)
    another operation x1, other arithmetic, local_map(): solved = jax.scipy.linalg.solve_triangular(system, right_side, lower=True)  158 us
    unnamed x4, waiting for transfers between devices  55.5 us
    all_gather x1, waiting for transfers between devices, entering(): everything = lax.all_gather(shard, axis)  30.5 us
    reduce_scatter x1, waiting for transfers between devices, per_device(): lax.psum_scatter(own_term, 'sp', scatter_dimension=3, tiled=True)  19.3 us
    dot_general x8, matrix products, advance(): jnp.einsum('shck,shcv->shkv', carried_now, value_now, precision=highest)  12.1 us
    dot_general x8, matrix products, advance(): mixed = jnp.einsum('shck,shkx->shcx', key_now, carry_map, precision=highest)  10.7 us
    psum x1, blocking collectives, per_device(): squares = lax.psum(jnp.sum(readout * readout, axis=-1), 'sp')  8.73 us
    dot_general x5, matrix products, compose(): return jnp.einsum('shij,shjk->shik', earlier, later, precision=highest)  7.32 us
  transfers between devices with their start and end apart: 3, of which 3 were waited for; matrix products, arithmetic and copies ran while one was open for 1% of the time, Pallas kernels for 0%

commit v1 on v0

v1 whole, which is shorter than its diff:
```python
import functools

import jax
import jax.numpy as jnp
from jax import lax
from jax.experimental import pallas as pl
from jax.experimental.pallas import tpu as pltpu
from jax.sharding import PartitionSpec as P

DK = 128
SPAN = 128
MESH = pl.DeviceIdType.MESH

epsilon = 1e-06
highest = lax.Precision.HIGHEST
F32 = jnp.float32
BF16 = jnp.bfloat16
NN = (((1,), (0,)), ((), ()))
NT = (((1,), (1,)), ((), ()))
TN = (((0,), (0,)), ((), ()))


def mm(a, b, dims=NN, precision=None):
    return lax.dot_general(a, b, dims, precision=precision, preferred_element_type=F32)


def bf(a):
    return a.astype(BF16)


def split(a):
    high = bf(a)
    return high, bf(a - high.astype(F32))


def mm3(a, b, dims=NN):
    a_high, a_low = a
    b_high, b_low = b
    return mm(a_high, b_high, dims) + (mm(a_high, b_low, dims) + mm(a_low, b_high, dims))


def softplus(a):
    return jnp.maximum(a, 0.0) + jnp.log1p(jnp.exp(-jnp.abs(a)))


def row_of(scalars, width):
    lanes = lax.broadcasted_iota(jnp.int32, (1, width), 1)
    row = jnp.zeros((1, width), F32)
    for j in range(width):
        row = jnp.where(lanes == j, scalars[j], row)
    return row


def map_kernel(heads, rate_ref, shift_ref, x_ref, wk_ref, wv_ref, wb_ref, wd_ref, extra_ref, map_ref):
    length = x_ref.shape[1]
    head_total = wb_ref.shape[1]
    chunks = length // SPAN
    first = lax.axis_index("tp") * heads
    x = x_ref[0]
    kb = bf(mm(x, wk_ref[...]))
    vb = bf(mm(x, wv_ref[...]))
    beta_all = jax.nn.sigmoid(bf(mm(x, wb_ref[...])).astype(F32) + row_of(shift_ref, head_total))
    soft_all = softplus(bf(mm(x, wd_ref[...])).astype(F32)) * -row_of(rate_ref, head_total)
    head_lanes = lax.broadcasted_iota(jnp.int32, (length, head_total), 1)

    lanes = lax.broadcasted_iota(jnp.int32, (SPAN, SPAN), 1)
    rows = lax.broadcasted_iota(jnp.int32, (SPAN, SPAN), 0)
    strict = rows > lanes
    apart = rows ^ lanes
    eye = jnp.where(rows == lanes, 1.0, 0.0)
    tri = jnp.where(rows >= lanes, 1.0, 0.0)

    count = heads * chunks
    combos = [(h, n) for h in range(heads) for n in range(chunks)]
    log_matrix = jnp.zeros((SPAN, SPAN), F32)
    other = jnp.zeros((SPAN, SPAN), F32)
    betas, norms = [], []
    for h in range(heads):
        here = head_lanes == first + h
        beta = jnp.sum(jnp.where(here, beta_all, 0.0), axis=1, keepdims=True)
        log_decay = jnp.sum(jnp.where(here, soft_all, 0.0), axis=1, keepdims=True)
        log_decay = log_decay + extra_ref[0, :, h : h + 1]
        keys = kb[:, h * DK : (h + 1) * DK].astype(F32)
        inverse_norm = lax.rsqrt(jnp.sum(keys * keys, axis=1, keepdims=True) + epsilon)
        for n in range(chunks):
            c = h * chunks + n
            part = slice(n * SPAN, (n + 1) * SPAN)
            log_matrix = jnp.where(lanes == c, log_decay[part], log_matrix)
            other = jnp.where(lanes == count + c, beta[part], other)
            other = jnp.where(lanes == 2 * count + c, inverse_norm[part], other)
            betas.append(beta[part])
            norms.append(inverse_norm[part])
    cumulative = mm(tri, log_matrix, precision=highest)
    by_row = jnp.where(lanes < count, cumulative, other).T

    keys, lowers, inverses = [], [], []
    for c, (h, n) in enumerate(combos):
        kr = kb[n * SPAN : (n + 1) * SPAN, h * DK : (h + 1) * DK]
        spread = cumulative[:, c : c + 1] - by_row[c : c + 1]
        decay = jnp.exp(jnp.where(strict, spread, 0.0))
        scale = (betas[c] * norms[c]) * by_row[2 * count + c : 2 * count + c + 1]
        lower = jnp.where(strict, mm(kr, kr, NT) * scale * decay, 0.0)
        keys.append(kr)
        lowers.append(lower)
        inverses.append(eye - jnp.where(apart < 2, lower, 0.0))
    size = 2
    while size < SPAN:
        level = (apart >= size) & (apart < 2 * size)
        narrow = [bf(inverse) for inverse in inverses]
        steps = [mm(bf(jnp.where(level, lower, 0.0)), x1) for lower, x1 in zip(lowers, narrow)]
        inverses = [
            inverse - mm(x1, bf(step)) for inverse, x1, step in zip(inverses, narrow, steps)
        ]
        size *= 2

    decays, pieces = [], []
    for c, (h, n) in enumerate(combos):
        values = vb[n * SPAN : (n + 1) * SPAN, h * DK : (h + 1) * DK]
        last = cumulative[SPAN - 1 : SPAN, c : c + 1]
        beta_row = by_row[count + c : count + c + 1]
        key_row = beta_row * by_row[2 * count + c : 2 * count + c + 1] * jnp.exp(by_row[c : c + 1])
        carry = norms[c] * jnp.exp(last - cumulative[:, c : c + 1])
        key_part = mm(bf(inverses[c] * key_row), keys[c]) * carry
        value_part = mm(bf(inverses[c] * beta_row), values) * carry
        both = bf(jnp.concatenate([key_part, value_part], axis=1))
        pieces.append(mm(both, keys[c], TN))
        decays.append(jnp.exp(last))
    for h in range(heads):
        c = h * chunks
        key_map, offset = pieces[c][:DK], pieces[c][DK:]
        linear = eye * decays[c] - key_map
        for n in range(1, chunks):
            c = h * chunks + n
            key_map = bf(pieces[c][:DK])
            linear = linear * decays[c] - mm(bf(linear), key_map)
            offset = offset * decays[c] - mm(bf(offset), key_map) + pieces[c][DK:]
        map_ref[0, h, :DK] = linear
        map_ref[0, h, DK:] = offset


def chain_kernel(
    sp_size,
    tp_size,
    map_ref,
    query_ref,
    gate_ref,
    gain_ref,
    weight_ref,
    cache_ref,
    out_ref,
    state_in,
    state_out,
    cols_send,
    cols_recv,
    norm_send,
    norm_recv,
    part_send,
    part_recv,
    chain_send_sem,
    chain_recv_sem,
    cols_send_sem,
    cols_recv_sem,
    norm_send_sem,
    norm_recv_sem,
    part_send_sem,
    part_recv_sem,
):
    seqs, heads = map_ref.shape[:2]
    columns = weight_ref.shape[1]
    features = part_send.shape[2]
    devices = sp_size * tp_size
    last = sp_size - 1
    me = lax.axis_index("sp")
    tp_here = lax.axis_index("tp")
    rank = me * tp_size + tp_here
    unroll = devices <= 16

    def where(target):
        return {"sp": target // tp_size, "tp": target % tp_size}

    def each_other(body):
        def turn(step, carry):
            body(step, lax.rem(rank + step, devices))
            return carry

        lax.fori_loop(1, devices, turn, 0, unroll=unroll)

    barrier = pltpu.get_barrier_semaphore()
    each_other(
        lambda step, target: pl.semaphore_signal(
            barrier, inc=1, device_id=where(target), device_id_type=MESH
        )
    )
    pl.semaphore_wait(barrier, devices - 1)

    def chain_copy(p, target):
        return pltpu.make_async_remote_copy(
            src_ref=state_out.at[p],
            dst_ref=state_in.at[p],
            send_sem=chain_send_sem.at[p],
            recv_sem=chain_recv_sem.at[p],
            device_id={"sp": target},
            device_id_type=MESH,
        )

    def cols_copy(p, d):
        return pltpu.make_async_remote_copy(
            src_ref=cols_send.at[d, p],
            dst_ref=cols_recv.at[p],
            send_sem=cols_send_sem.at[d, p],
            recv_sem=cols_recv_sem.at[p],
            device_id={"sp": d},
            device_id_type=MESH,
        )

    def norm_copy(d):
        return pltpu.make_async_remote_copy(
            src_ref=norm_send,
            dst_ref=norm_recv,
            send_sem=norm_send_sem.at[d],
            recv_sem=norm_recv_sem,
            device_id={"sp": d},
            device_id_type=MESH,
        )

    @pl.when(me == last)
    def _():
        norm_send[...] = jnp.zeros_like(norm_send)

    queries = query_ref[...].astype(F32)
    gates = jax.nn.silu(gate_ref[...].astype(F32))
    for s in range(seqs):
        for h in range(heads):
            p = h * seqs + s

            @pl.when(me == 0)
            def _():
                state_out[p] = map_ref[s, h, DK:]

            @pl.when(me > 0)
            def _():
                linear = split(map_ref[s, h, :DK])
                chain_copy(p, 0).wait_recv()
                state_out[p] = mm3(split(state_in[p]), linear) + map_ref[s, h, DK:]

            @pl.when(me < last)
            def _():
                chain_copy(p, me + 1).start()

            @pl.when(me == last)
            def _():
                state = state_out[p]
                for d in range(sp_size):
                    cols_send[d, p] = state[d * columns : (d + 1) * columns]
                for d in range(last):
                    cols_copy(p, d).start()
                cols_recv[p] = state[last * columns :]
                query = queries[s : s + 1, h * DK : (h + 1) * DK]
                query = query * lax.rsqrt(
                    jnp.sum(query * query, axis=1, keepdims=True) + epsilon
                ) * DK ** (-0.5)
                readout = mm(query, state, NT, highest)
                mean = jnp.mean(readout * readout, axis=1, keepdims=True)
                scaled = readout * lax.rsqrt(mean + epsilon)
                gate = gates[s : s + 1, h * DK : (h + 1) * DK]
                norm_send[p : p + 1] = bf(scaled * gain_ref[...] * gate).astype(F32)

    @pl.when(me == last)
    def _():
        for d in range(last):
            norm_copy(d).start()
        norm_recv[...] = norm_send[...]

    @pl.when(me < last)
    def _():
        for p in range(seqs * heads):
            chain_copy(p, me + 1).wait_send()
        norm_copy(0).wait_recv()

    picked = (
        lax.broadcasted_iota(jnp.int32, (DK, columns), 0)
        == lax.broadcasted_iota(jnp.int32, (DK, columns), 1) + me * columns
    )
    normed = bf(mm(bf(norm_recv[...]), bf(jnp.where(picked, 1.0, 0.0))))
    partial = mm(normed[:seqs], weight_ref[0])
    for h in range(1, heads):
        partial = partial + mm(normed[h * seqs : (h + 1) * seqs], weight_ref[h])
    for j in range(devices):
        part_send[j] = partial[:, j * features : (j + 1) * features]

    def part_copy(step, target, slot):
        return pltpu.make_async_remote_copy(
            src_ref=part_send.at[target],
            dst_ref=part_recv.at[slot],
            send_sem=part_send_sem.at[step],
            recv_sem=part_recv_sem.at[slot],
            device_id=where(target),
            device_id_type=MESH,
        )

    each_other(lambda step, target: part_copy(step, target, rank).start())
    part_recv[rank] = part_send[rank]

    @pl.when(me < last)
    def _():
        for p in range(seqs * heads):
            cols_copy(p, 0).wait_recv()

    eye = bf(
        jnp.where(
            lax.broadcasted_iota(jnp.int32, (DK, DK), 0)
            == lax.broadcasted_iota(jnp.int32, (DK, DK), 1),
            1.0,
            0.0,
        )
    )
    for s in range(seqs):
        for h in range(heads):
            cache_ref[s, h] = bf(mm(eye, bf(cols_recv[h * seqs + s]), NT))

    each_other(lambda step, target: part_copy(step, target, target).wait_recv())

    def add(j, total):
        return total + part_recv[j]

    out_ref[...] = lax.fori_loop(0, devices, add, jnp.zeros(out_ref.shape, F32), unroll=unroll)

    each_other(lambda step, target: part_copy(step, target, rank).wait_send())

    @pl.when(me == last)
    def _():
        for d in range(last):
            norm_copy(d).wait_send()
            for p in range(seqs * heads):
                cols_copy(p, d).wait_send()


def per_device(
    sp_size,
    tp_size,
    layer_input,
    key_weight,
    value_weight,
    beta_weight,
    beta_shift,
    decay_weight,
    decay_rate,
    decay_extra,
    query_new,
    gate_new,
    norm_gain,
    out_weight,
):
    seqs, length, width = layer_input.shape
    heads = key_weight.shape[1] // DK
    columns = out_weight.shape[1]
    devices = sp_size * tp_size
    features = out_weight.shape[2] // devices
    pairs = seqs * heads
    norm_rows = -(-pairs // 8) * 8
    whole = lambda array: pl.BlockSpec(array.shape, lambda s: (0,) * array.ndim)
    smem = pl.BlockSpec(memory_space=pltpu.SMEM)
    vmem = pl.BlockSpec(memory_space=pltpu.VMEM)
    maps = pl.pallas_call(
        functools.partial(map_kernel, heads),
        grid=(seqs,),
        in_specs=[
            smem,
            smem,
            pl.BlockSpec((1, length, width), lambda s: (s, 0, 0)),
            whole(key_weight),
            whole(value_weight),
            whole(beta_weight),
            whole(decay_weight),
            pl.BlockSpec((1, length, heads), lambda s: (s, 0, 0)),
        ],
        out_specs=pl.BlockSpec((1, heads, 2 * DK, DK), lambda s: (s, 0, 0, 0)),
        out_shape=jax.ShapeDtypeStruct((seqs, heads, 2 * DK, DK), F32),
        compiler_params=pltpu.CompilerParams(vmem_limit_bytes=48 * 1024 * 1024),
    )(
        decay_rate,
        beta_shift,
        layer_input,
        key_weight,
        value_weight,
        beta_weight,
        decay_weight,
        decay_extra,
    )
    dma = pltpu.SemaphoreType.DMA
    return pl.pallas_call(
        functools.partial(chain_kernel, sp_size, tp_size),
        in_specs=[vmem] * 5,
        out_specs=(vmem, vmem),
        out_shape=(
            jax.ShapeDtypeStruct((seqs, heads, DK, columns), BF16),
            jax.ShapeDtypeStruct((seqs, features), F32),
        ),
        scratch_shapes=[
            pltpu.VMEM((pairs, DK, DK), F32),
            pltpu.VMEM((pairs, DK, DK), F32),
            pltpu.VMEM((sp_size, pairs, columns, DK), F32),
            pltpu.VMEM((pairs, columns, DK), F32),
            pltpu.VMEM((norm_rows, DK), F32),
            pltpu.VMEM((norm_rows, DK), F32),
            pltpu.VMEM((devices, seqs, features), F32),
            pltpu.VMEM((devices, seqs, features), F32),
            dma((pairs,)),
            dma((pairs,)),
            dma((sp_size, pairs)),
            dma((pairs,)),
            dma((sp_size,)),
            dma,
            dma((devices,)),
            dma((devices,)),
        ],
        compiler_params=pltpu.CompilerParams(collective_id=0, has_side_effects=True),
    )(maps, query_new, gate_new, norm_gain.reshape(1, DK), out_weight)


def solution(mesh):
    return jax.shard_map(
        functools.partial(per_device, mesh.shape["sp"], mesh.shape["tp"]),
        mesh=mesh,
        in_specs=(
            P("grp", "sp", None),
            P(None, "tp"),
            P(None, "tp"),
            P(),
            P(),
            P(),
            P(),
            P("grp", "sp", "tp"),
            P("grp", "tp"),
            P("grp", "tp"),
            P(),
            P("tp", "sp", None),
        ),
        out_specs=(P("grp", "tp", None, "sp"), P("grp", ("sp", "tp"))),
        check_vma=False,
    )
```

time: 357 us -> 55.8 us (0.16)
  other arithmetic: 164 us -> 0 us
  waiting for transfers between devices: 105 us -> 0 us
  matrix products: 56.7 us -> 0 us
  Pallas kernels: 0 us -> 44.3 us
  between operations: 14 us -> 0.69 us
  blocking collectives: 8.73 us -> 0 us
    another operation x2 -> x0, other arithmetic: 159 us -> none  [the longest x1 158 us: local_map(): solved = jax.scipy.linalg.solve_triangular(system, right_side, lower=True)]
    unnamed x4 -> x0, waiting for transfers between devices: 55.5 us -> none
    dot_general x36 -> x0, matrix products: 54.7 us -> none  [the longest x8 12.1 us: advance(): jnp.einsum('shck,shcv->shkv', carried_now, value_now, precision=highest)]
    pallas_call x0 -> x2, Pallas kernels: none -> 44.3 us  [the longest x1 29.9 us: per_device(): pl.pallas_call(functools.partial(chain_kernel, sp_size, tp_size), in_spec...]
    all_gather x1 -> x0, waiting for transfers between devices: 30.5 us -> none  [entering(): everything = lax.all_gather(shard, axis)]
    reduce_scatter x1 -> x0, waiting for transfers between devices: 19.3 us -> none  [per_device(): lax.psum_scatter(own_term, 'sp', scatter_dimension=3, tiled=True)]
    psum x1 -> x0, blocking collectives: 8.73 us -> none  [per_device(): squares = lax.psum(jnp.sum(readout * readout, axis=-1), 'sp')]
    unnamed x16 -> x14, local copies, waits for them, and re-layouts: 1.6 us -> 8.73 us
  transfers between devices with their start and end apart: 3 -> 0, of which waited for: 3 -> 0; matrix products, arithmetic and copies ran while one was open for 1% -> 0% of each run, Pallas kernels for 0% -> 0%
where the time goes in v1:
time: 55.8 us; the launch traced here: 55.4 us
  Pallas kernels  44.3 us (79%)
  local copies, waits for them, and re-layouts  10.3 us (18%)
  between operations  0.69 us (1%)
    pallas_call x1, Pallas kernels, per_device(): pl.pallas_call(functools.partial(chain_kernel, sp_size, tp_size), in_spec...  29.9 us
    pallas_call x1, Pallas kernels, per_device(): pl.pallas_call(functools.partial(map_kernel, heads), grid=(seqs,), in_spe...  14.4 us
    unnamed x14, local copies, waits for them, and re-layouts  8.73 us
    pallas_call x1, local copies, waits for them, and re-layouts, per_device(): pl.pallas_call(functools.partial(chain_kernel, sp_size, tp_size), in_spec...  1.6 us

profile of v1, /device:TPU:0, one launch (start us, length us, event | category | flops | bytes accessed | tf_op | source)
XLA Modules:
  0.0 55.4 jit_solution(4291159033988692140)
XLA Ops:
  0.6 1.0 %copy.14.wb_ref = bf16[2048,8]{1,0:T(8,128)(2,1)S(1)} copy(bf16[2048,8]{0,1:T(8,128)(2,1)} %param.15) | data formatting | bytes 65536 | tf_op args[3]
  1.7 1.0 %copy.15.wd_ref = bf16[2048,8]{1,0:T(8,128)(2,1)S(1)} copy(bf16[2048,8]{0,1:T(8,128)(2,1)} %param.17) | data formatting | bytes 65536 | tf_op args[5]
  2.7 0.9 %copy.16.extra_ref = f32[2,512,2]{2,1,0:T(8,128)S(1)} copy(f32[2,512,2]{1,2,0:T(2,128)} %param.19) | data formatting | bytes 16384 | tf_op args[7]
  3.6 0.0 copy-start.1
  3.6 1.2 %copy-done.1 = bf16[2048,256]{1,0:T(8,128)(2,1)S(1)} copy-done((bf16[2048,256]{1,0:T(8,128)(2,1)S(1)}, bf16[2048,256]{1,0:T(8,128)(2,1)}, u32[]{:S(2)}) %copy-start.1) | copy-done | bytes 1048600
  4.9 0.0 copy-start.2
  4.9 1.2 %copy-done.2 = bf16[2048,256]{1,0:T(8,128)(2,1)S(1)} copy-done((bf16[2048,256]{1,0:T(8,128)(2,1)S(1)}, bf16[2048,256]{1,0:T(8,128)(2,1)}, u32[]{:S(2)}) %copy-start.2) | copy-done | bytes 1048600
  6.1 0.0 copy-start.3
  6.1 0.7 %copy-done.3 = f32[8]{0:T(128)S(1)} copy-done((f32[8]{0:T(128)S(1)}, f32[8]{0:T(128)}, u32[]{:S(2)}) %copy-start.3) | copy-done | bytes 56
  6.7 0.0 copy-start.4
  6.7 0.7 %copy-done.4 = f32[8]{0:T(128)S(1)} copy-done((f32[8]{0:T(128)S(1)}, f32[8]{0:T(128)}, u32[]{:S(2)}) %copy-start.4) | copy-done | bytes 56
  7.4 14.4 %shard_map.131.map_ref = f32[2,2,256,128]{3,2,1,0:T(8,128)S(1)} custom-call(f32[8]{0:T(128)S(1)} %copy-done.3, f32[8]{0:T(128)S(1)} %copy-done.4, bf16[2,512,2048]{2,1,0:T(8,128)(2,1)} %x_ref.1, bf16[2048,256]{1,0:T(8,128)(2,1)S(1)} %copy-done.1, bf16[2048,256]{1,0:T(8,128)(2,1)S(1)} %copy-done.2, bf16[2048,8]{1,0:T(8,128)(2,1)S(1)} %copy.14.wb_ref, ...), custom_call_target="tpu_custom_call" | custom-call | tf_op jit(solution)/shard_map/pallas_call | solution.py:364
  21.8 0.0 copy-start
  21.9 0.8 %copy-done = f32[2,2,256,128]{3,2,1,0:T(8,128)} copy-done((f32[2,2,256,128]{3,2,1,0:T(8,128)}, f32[2,2,256,128]{3,2,1,0:T(8,128)S(1)}, u32[]{:S(2)}) %copy-start) | copy-done | bytes 524312
  22.6 29.9 %shard_map.132 = (bf16[2,2,128,32]{3,2,1,0:T(8,128)(2,1)}, f32[2,128]{1,0:T(2,128)}) custom-call(f32[2,2,256,128]{3,2,1,0:T(8,128)} %copy-done, bf16[2,256]{1,0:T(2,128)(2,1)} %query_ref.1, bf16[2,256]{1,0:T(2,128)(2,1)} %gate_ref.1, f32[1,128]{1,0:T(1,128)} %bitcast.1, bf16[2,32,2048]{2,1,0:T(8,128)(2,1)} %weight_ref.1), custom_call_target="tpu_custom_call" | custom-call | tf_op jit(solution)/shard_map/pallas_call | solution.py:391
  52.5 1.6 %copy.17 = bf16[2,2,128,32]{2,3,1,0:T(8,128)(2,1)} copy(bf16[2,2,128,32]{3,2,1,0:T(8,128)(2,1)} %get-tuple-element.2) | data formatting | bytes 65536 | tf_op jit(solution)/shard_map/pallas_call | solution.py:391
  54.1 1.2 %copy.19 = f32[2,128]{1,0:T(2,128)} copy(f32[2,128]{1,0:T(2,128)} %get-tuple-element.7) | data formatting | bytes 2048
Async XLA Ops:
  3.6 1.2 %copy-start.1 = (bf16[2048,256]{1,0:T(8,128)(2,1)S(1)}, bf16[2048,256]{1,0:T(8,128)(2,1)}, u32[]{:S(2)}) copy-start(bf16[2048,256]{1,0:T(8,128)(2,1)} %wk_ref.1) | copy-start | bytes 3145732
  4.9 1.2 %copy-start.2 = (bf16[2048,256]{1,0:T(8,128)(2,1)S(1)}, bf16[2048,256]{1,0:T(8,128)(2,1)}, u32[]{:S(2)}) copy-start(bf16[2048,256]{1,0:T(8,128)(2,1)} %wv_ref.1) | copy-start | bytes 3145732
  6.1 0.7 %copy-start.3 = (f32[8]{0:T(128)S(1)}, f32[8]{0:T(128)}, u32[]{:S(2)}) copy-start(f32[8]{0:T(128)} %rate_ref.1) | copy-start | bytes 100
  6.7 0.7 %copy-start.4 = (f32[8]{0:T(128)S(1)}, f32[8]{0:T(128)}, u32[]{:S(2)}) copy-start(f32[8]{0:T(128)} %shift_ref.1) | copy-start | bytes 100
  21.8 0.8 %copy-start = (f32[2,2,256,128]{3,2,1,0:T(8,128)}, f32[2,2,256,128]{3,2,1,0:T(8,128)S(1)}, u32[]{:S(2)}) copy-start(f32[2,2,256,128]{3,2,1,0:T(8,128)S(1)} %shard_map.131.map_ref) | copy-start | bytes 1572868

commit v2 on v1

v2 whole, which is shorter than its diff:
```python
import functools

import jax
import jax.numpy as jnp
from jax import lax
from jax.experimental import pallas as pl
from jax.experimental.pallas import tpu as pltpu
from jax.sharding import PartitionSpec as P

DK = 128
SPAN = 128
MESH = pl.DeviceIdType.MESH

epsilon = 1e-06
highest = lax.Precision.HIGHEST
F32 = jnp.float32
BF16 = jnp.bfloat16
NN = (((1,), (0,)), ((), ()))
NT = (((1,), (1,)), ((), ()))
TN = (((0,), (0,)), ((), ()))


def mm(a, b, dims=NN, precision=None):
    return lax.dot_general(a, b, dims, precision=precision, preferred_element_type=F32)


def bf(a):
    return a.astype(BF16)


def split(a):
    high = bf(a)
    return high, bf(a - high.astype(F32))


def mm3(a, b, dims=NN):
    a_high, a_low = a
    b_high, b_low = b
    return mm(a_high, b_high, dims) + (mm(a_high, b_low, dims) + mm(a_low, b_high, dims))


def softplus(a):
    return jnp.maximum(a, 0.0) + jnp.log1p(jnp.exp(-jnp.abs(a)))


def column_of(row):
    width = row.shape[1]
    rows = lax.broadcasted_iota(jnp.int32, (width, width), 0)
    lanes = lax.broadcasted_iota(jnp.int32, (width, width), 1)
    return jnp.sum(jnp.where(rows == lanes, row, 0.0), axis=1, keepdims=True)


def segment_maps(x, wk, wv, small_weights, rate_row, shift_row, extra, heads, first):
    length = x.shape[0]
    head_total = rate_row.shape[1]
    chunks = length // SPAN
    kb = bf(mm(x, wk))
    vb = bf(mm(x, wv))
    raw = bf(mm(small_weights, x, NT)).astype(F32)
    beta_all = jax.nn.sigmoid(raw[:head_total] + column_of(shift_row))
    soft_all = softplus(raw[head_total:]) * -column_of(rate_row)
    head_rows = lax.broadcasted_iota(jnp.int32, (head_total, length), 0)

    lanes = lax.broadcasted_iota(jnp.int32, (SPAN, SPAN), 1)
    rows = lax.broadcasted_iota(jnp.int32, (SPAN, SPAN), 0)
    strict = rows > lanes
    diagonal = rows == lanes
    apart = rows ^ lanes
    eye = jnp.where(diagonal, 1.0, 0.0)
    upper = jnp.where(rows <= lanes, 1.0, 0.0)

    combos = [(h, n) for h in range(heads) for n in range(chunks)]
    count = -(-len(combos) // 8) * 8
    places = lax.broadcasted_iota(jnp.int32, (count, SPAN), 0)
    logs = jnp.zeros((count, SPAN), F32)
    betas = jnp.zeros((count, SPAN), F32)
    norms = jnp.zeros((count, SPAN), F32)
    keys, products = [], []
    for h in range(heads):
        here = head_rows == first + h
        beta = jnp.sum(jnp.where(here, beta_all, 0.0), axis=0, keepdims=True)
        log_decay = jnp.sum(jnp.where(here, soft_all, 0.0), axis=0, keepdims=True)
        log_decay = log_decay + extra[h : h + 1]
        for n in range(chunks):
            c = h * chunks + n
            part = slice(n * SPAN, (n + 1) * SPAN)
            kr = kb[part, h * DK : (h + 1) * DK]
            product = mm(kr, kr, NT)
            squares = jnp.sum(jnp.where(diagonal, product, 0.0), axis=0, keepdims=True)
            logs = jnp.where(places == c, log_decay[:, part], logs)
            betas = jnp.where(places == c, beta[:, part], betas)
            norms = jnp.where(places == c, lax.rsqrt(squares + epsilon), norms)
            keys.append(kr)
            products.append(product)
    cumulative = mm(logs, upper, precision=highest)
    last_logs = cumulative[:, SPAN - 1 :]
    key_rows = betas * norms * jnp.exp(cumulative)
    carries = norms * jnp.exp(last_logs - cumulative)
    stacked = [cumulative, betas * norms, carries]
    if 3 * count < SPAN:
        stacked.append(jnp.zeros((SPAN - 3 * count, SPAN), F32))
    by_column = jnp.concatenate(stacked, axis=0).T
    block_decays = jnp.exp(last_logs)

    lowers, inverses = [], []
    for c in range(len(combos)):
        spread = by_column[:, c : c + 1] - cumulative[c : c + 1]
        scale = by_column[:, count + c : count + c + 1] * norms[c : c + 1]
        decay = jnp.exp(jnp.where(strict, spread, 0.0))
        lower = jnp.where(strict, products[c] * scale * decay, 0.0)
        lowers.append(lower)
        inverses.append(eye - jnp.where(apart < 2, lower, 0.0))
    size = 2
    while size < SPAN:
        level = (apart >= size) & (apart < 2 * size)
        narrow = [bf(inverse) for inverse in inverses]
        steps = [mm(bf(jnp.where(level, lower, 0.0)), x1) for lower, x1 in zip(lowers, narrow)]
        inverses = [
            inverse - mm(x1, bf(step)) for inverse, x1, step in zip(inverses, narrow, steps)
        ]
        size *= 2

    pieces = []
    for c, (h, n) in enumerate(combos):
        values = vb[n * SPAN : (n + 1) * SPAN, h * DK : (h + 1) * DK]
        carry = by_column[:, 2 * count + c : 2 * count + c + 1]
        key_part = mm(bf(inverses[c] * key_rows[c : c + 1]), keys[c]) * carry
        value_part = mm(bf(inverses[c] * betas[c : c + 1]), values) * carry
        both = bf(jnp.concatenate([key_part, value_part], axis=1))
        pieces.append(mm(both, keys[c], TN))
    maps = []
    for h in range(heads):
        c = h * chunks
        linear = eye * block_decays[c : c + 1] - pieces[c][:DK]
        offset = pieces[c][DK:]
        for n in range(1, chunks):
            c = h * chunks + n
            fading = block_decays[c : c + 1]
            key_map = bf(pieces[c][:DK])
            linear = linear * fading - mm(bf(linear), key_map)
            offset = offset * fading - mm(bf(offset), key_map) + pieces[c][DK:]
        maps.append((linear, offset))
    return maps


def mixer_kernel(
    sp_size,
    tp_size,
    x_hbm,
    wk_hbm,
    wv_hbm,
    wb_ref,
    wd_ref,
    shift_ref,
    rate_ref,
    extra_ref,
    query_ref,
    gate_ref,
    gain_ref,
    weight_ref,
    cache_ref,
    out_ref,
    x_ref,
    wk_ref,
    wv_ref,
    maps,
    state_in,
    state_out,
    cols_send,
    cols_recv,
    back_in,
    back_out,
    norm_send,
    norm_recv,
    part_send,
    part_recv,
    load_sem,
    chain_send_sem,
    chain_recv_sem,
    cols_send_sem,
    cols_recv_sem,
    back_sem,
    norm_send_sem,
    norm_recv_sem,
    part_send_sem,
    part_recv_sem,
):
    seqs, heads = maps.shape[:2]
    pairs = seqs * heads
    columns = weight_ref.shape[1]
    features = part_send.shape[2]
    devices = sp_size * tp_size
    last = sp_size - 1
    half = DK // 2
    me = lax.axis_index("sp")
    tp_here = lax.axis_index("tp")
    rank = me * tp_size + tp_here
    unroll = devices <= 16

    def where(target):
        return {"sp": target // tp_size, "tp": target % tp_size}

    def each_other(body):
        def turn(step, carry):
            body(step, lax.rem(rank + step, devices))
            return carry

        lax.fori_loop(1, devices, turn, 0, unroll=unroll)

    loads = [
        pltpu.make_async_copy(wk_hbm, wk_ref, load_sem.at[0]),
        pltpu.make_async_copy(wv_hbm, wv_ref, load_sem.at[1]),
    ]
    loads += [
        pltpu.make_async_copy(x_hbm.at[s], x_ref.at[s], load_sem.at[2 + s]) for s in range(seqs)
    ]
    for load in (loads[0], loads[2], loads[1], *loads[3:]):
        load.start()
    barrier = pltpu.get_barrier_semaphore()
    each_other(
        lambda step, target: pl.semaphore_signal(
            barrier, inc=1, device_id=where(target), device_id_type=MESH
        )
    )

    def chain_copy(p, t, target):
        return pltpu.make_async_remote_copy(
            src_ref=state_out.at[p, t],
            dst_ref=state_in.at[p, t],
            send_sem=chain_send_sem.at[p, t],
            recv_sem=chain_recv_sem.at[p, t],
            device_id={"sp": target},
            device_id_type=MESH,
        )

    def cols_copy(p, d):
        return pltpu.make_async_remote_copy(
            src_ref=cols_send.at[d, p],
            dst_ref=cols_recv.at[p],
            send_sem=cols_send_sem.at[d, p],
            recv_sem=cols_recv_sem.at[p],
            device_id={"sp": d},
            device_id_type=MESH,
        )

    def back_copy(target):
        return pltpu.make_async_remote_copy(
            src_ref=back_out,
            dst_ref=back_in,
            send_sem=back_sem.at[0],
            recv_sem=back_sem.at[1],
            device_id={"sp": target},
            device_id_type=MESH,
        )

    def norm_copy(d):
        return pltpu.make_async_remote_copy(
            src_ref=norm_send,
            dst_ref=norm_recv,
            send_sem=norm_send_sem.at[d],
            recv_sem=norm_recv_sem,
            device_id={"sp": d},
            device_id_type=MESH,
        )

    def part_copy(step, target, slot):
        return pltpu.make_async_remote_copy(
            src_ref=part_send.at[target],
            dst_ref=part_recv.at[slot],
            send_sem=part_send_sem.at[step],
            recv_sem=part_recv_sem.at[slot],
            device_id=where(target),
            device_id_type=MESH,
        )

    small_weights = jnp.concatenate([wb_ref[...], wd_ref[...]], axis=0)
    for load in (loads[0], loads[1]):
        load.wait()
    for s in range(seqs):
        loads[2 + s].wait()
        found = segment_maps(
            x_ref[s],
            wk_ref[...],
            wv_ref[...],
            small_weights,
            rate_ref[...],
            shift_ref[...],
            extra_ref[s],
            heads,
            tp_here * heads,
        )
        for h in range(heads):
            maps[s, h, :DK] = found[h][0]
            maps[s, h, DK:] = found[h][1]
        if s == 0:
            pl.semaphore_wait(barrier, devices - 1)

        @pl.when(me == 0)
        def _():
            for h in range(heads):
                p = s * heads + h
                for t in range(2):
                    state_out[p, t] = maps[s, h, DK + t * half : DK + (t + 1) * half]
                    chain_copy(p, t, 1).start()

    def back_step():
        @pl.when(me == last)
        def _():
            queries = query_ref[...].astype(F32)
            back_in[...] = jnp.zeros_like(back_in)
            for s in range(seqs):
                for h in range(heads):
                    query = queries[s : s + 1, h * DK : (h + 1) * DK]
                    size = jnp.sum(query * query, axis=1, keepdims=True) + epsilon
                    row = s * heads + h
                    back_in[0, row : row + 1] = query * lax.rsqrt(size) * DK ** (-0.5)

        @pl.when(me < last)
        def _():
            back_copy(0).wait_recv()

        for s in range(seqs):
            for h in range(heads):
                row = s * heads + h
                query = split(back_in[0, row : row + 1])
                moved = mm3(query, split(maps[s, h]), NT)
                back_out[0, row : row + 1] = moved[:, :DK]
                back_out[1, row : row + 1] = back_in[1, row : row + 1] + moved[:, DK:]

        @pl.when(me > 0)
        def _():
            back_copy(me - 1).start()

        @pl.when(me == 0)
        def _():
            gates = jax.nn.silu(gate_ref[...].astype(F32))
            norm_send[...] = jnp.zeros_like(norm_send)
            for s in range(seqs):
                for h in range(heads):
                    row = s * heads + h
                    readout = back_out[1, row : row + 1]
                    mean = jnp.mean(readout * readout, axis=1, keepdims=True)
                    scaled = readout * lax.rsqrt(mean + epsilon)
                    gate = gates[s : s + 1, h * DK : (h + 1) * DK]
                    to = h * seqs + s
                    norm_send[to : to + 1] = bf(scaled * gain_ref[...] * gate).astype(F32)
            for d in range(1, sp_size):
                norm_copy(d).start()
            norm_recv[...] = norm_send[...]

    def out_step():
        @pl.when(me > 0)
        def _():
            norm_copy(0).wait_recv()

        picked = (
            lax.broadcasted_iota(jnp.int32, (DK, columns), 0)
            == lax.broadcasted_iota(jnp.int32, (DK, columns), 1) + me * columns
        )
        normed = bf(mm(bf(norm_recv[...]), bf(jnp.where(picked, 1.0, 0.0))))
        partial = mm(normed[:seqs], weight_ref[0])
        for h in range(1, heads):
            partial = partial + mm(normed[h * seqs : (h + 1) * seqs], weight_ref[h])
        for j in range(devices):
            part_send[j] = partial[:, j * features : (j + 1) * features]
        each_other(lambda step, target: part_copy(step, target, rank).start())
        part_recv[rank] = part_send[rank]

    def state_steps(chosen):
        @pl.when(me > 0)
        def _():
            for p in chosen:
                s, h = divmod(p, heads)
                linear = split(maps[s, h, :DK])
                for t in range(2):
                    offset = maps[s, h, DK + t * half : DK + (t + 1) * half]
                    chain_copy(p, t, 0).wait_recv()
                    state = mm3(split(state_in[p, t]), linear) + offset
                    state_out[p, t] = state

                    @pl.when(me < last)
                    def _():
                        chain_copy(p, t, me + 1).start()

                    @pl.when(me == last)
                    def _():
                        for d in range(t * half // columns, (t + 1) * half // columns):
                            at = d * columns - t * half
                            if d == last:
                                cols_recv[p] = state[at : at + columns]
                            else:
                                cols_send[d, p] = state[at : at + columns]
                                cols_copy(p, d).start()

    middle = pairs // 2
    late = 2 * me >= sp_size

    @pl.when(late)
    def _():
        back_step()

    state_steps(range(middle))

    @pl.when(jnp.logical_not(late))
    def _():
        back_step()

    @pl.when(me == last)
    def _():
        out_step()

    state_steps(range(middle, pairs))

    @pl.when(me < last)
    def _():
        out_step()

    each_other(lambda step, target: part_copy(step, target, target).wait_recv())

    def add(j, total):
        return total + part_recv[j]

    out_ref[...] = lax.fori_loop(0, devices, add, jnp.zeros(out_ref.shape, F32), unroll=unroll)

    @pl.when(me < last)
    def _():
        for p in range(pairs):
            for t in range(2):
                chain_copy(p, t, me + 1).wait_send()
            cols_copy(p, 0).wait_recv()

    for p in range(pairs):
        s, h = divmod(p, heads)
        cache_ref[s, h] = cols_recv[p]

    each_other(lambda step, target: part_copy(step, target, rank).wait_send())

    @pl.when(me == last)
    def _():
        for d in range(last):
            for p in range(pairs):
                cols_copy(p, d).wait_send()

    @pl.when(me > 0)
    def _():
        back_copy(me - 1).wait_send()

    @pl.when(me == 0)
    def _():
        for d in range(1, sp_size):
            norm_copy(d).wait_send()


def finish_kernel(cache_ref, out_ref, cache_out, out_out):
    cache_out[...] = bf(cache_ref[...])
    out_out[...] = out_ref[...]


def per_device(
    sp_size,
    tp_size,
    layer_input,
    key_weight,
    value_weight,
    beta_weight,
    beta_shift,
    decay_weight,
    decay_rate,
    decay_extra,
    query_new,
    gate_new,
    norm_gain,
    out_weight,
):
    seqs = layer_input.shape[0]
    heads = key_weight.shape[1] // DK
    head_total = beta_weight.shape[1]
    columns = out_weight.shape[1]
    devices = sp_size * tp_size
    features = out_weight.shape[2] // devices
    pairs = seqs * heads
    rows = -(-pairs // 8) * 8
    vmem = pl.BlockSpec(memory_space=pltpu.VMEM)
    anywhere = pl.BlockSpec(memory_space=pl.ANY)
    dma = pltpu.SemaphoreType.DMA
    states = jax.ShapeDtypeStruct((seqs, heads, columns, DK), F32)
    outs = jax.ShapeDtypeStruct((seqs, features), F32)
    cache, out = pl.pallas_call(
        functools.partial(mixer_kernel, sp_size, tp_size),
        in_specs=[anywhere] * 3 + [vmem] * 9,
        out_specs=(vmem, vmem),
        out_shape=(states, outs),
        scratch_shapes=[
            pltpu.VMEM(layer_input.shape, BF16),
            pltpu.VMEM(key_weight.shape, BF16),
            pltpu.VMEM(value_weight.shape, BF16),
            pltpu.VMEM((seqs, heads, 2 * DK, DK), F32),
            pltpu.VMEM((pairs, 2, DK // 2, DK), F32),
            pltpu.VMEM((pairs, 2, DK // 2, DK), F32),
            pltpu.VMEM((sp_size, pairs, columns, DK), F32),
            pltpu.VMEM((pairs, columns, DK), F32),
            pltpu.VMEM((2, rows, DK), F32),
            pltpu.VMEM((2, rows, DK), F32),
            pltpu.VMEM((rows, DK), F32),
            pltpu.VMEM((rows, DK), F32),
            pltpu.VMEM((devices, seqs, features), F32),
            pltpu.VMEM((devices, seqs, features), F32),
            dma((2 + seqs,)),
            dma((pairs, 2)),
            dma((pairs, 2)),
            dma((sp_size, pairs)),
            dma((pairs,)),
            dma((2,)),
            dma((sp_size,)),
            dma,
            dma((devices,)),
            dma((devices,)),
        ],
        compiler_params=pltpu.CompilerParams(
            collective_id=0, has_side_effects=True, vmem_limit_bytes=62 * 1024 * 1024
        ),
    )(
        layer_input,
        key_weight,
        value_weight,
        beta_weight.T,
        decay_weight.T,
        beta_shift.reshape(1, head_total),
        decay_rate.reshape(1, head_total),
        jnp.swapaxes(decay_extra, 1, 2),
        query_new,
        gate_new,
        norm_gain.reshape(1, DK),
        out_weight,
    )
    cache, out = pl.pallas_call(
        finish_kernel,
        in_specs=[vmem] * 2,
        out_specs=(vmem, vmem),
        out_shape=(jax.ShapeDtypeStruct(states.shape, BF16), outs),
    )(cache, out)
    return (jnp.swapaxes(cache, 2, 3), out)


def solution(mesh):
    return jax.shard_map(
        functools.partial(per_device, mesh.shape["sp"], mesh.shape["tp"]),
        mesh=mesh,
        in_specs=(
            P("grp", "sp", None),
            P(None, "tp"),
            P(None, "tp"),
            P(),
            P(),
            P(),
            P(),
            P("grp", "sp", "tp"),
            P("grp", "tp"),
            P("grp", "tp"),
            P(),
            P("tp", "sp", None),
        ),
        out_specs=(P("grp", "tp", None, "sp"), P("grp", ("sp", "tp"))),
        check_vma=False,
    )
```

time: 55.8 us -> 38.3 us (0.69)
  local copies, waits for them, and re-layouts: 10.3 us -> 0 us
  Pallas kernels: 44.3 us -> 37.5 us
    unnamed x14 -> x0, local copies, waits for them, and re-layouts: 8.73 us -> none
    pallas_call x2, Pallas kernels: 44.3 us -> 37.5 us  [the longest x1 36.1 us: per_device(): pl.pallas_call(functools.partial(mixer_kernel, sp_size, tp_size), in_spec...]
    pallas_call x1 -> x0, local copies, waits for them, and re-layouts: 1.6 us -> none  [per_device(): pl.pallas_call(functools.partial(chain_kernel, sp_size, tp_size), in_spec...]
where the time goes in v2:
time: 38.3 us; the launch traced here: 38.2 us
  Pallas kernels  37.5 us (98%)
  between operations  0.64 us (2%)
    pallas_call x1, Pallas kernels, per_device(): pl.pallas_call(functools.partial(mixer_kernel, sp_size, tp_size), in_spec...  36.1 us
    pallas_call x1, Pallas kernels, per_device(): pl.pallas_call(finish_kernel, in_specs=[vmem] * 2, out_specs=(vmem, vmem)...  1.47 us

profile of v2, /device:TPU:0, one launch (start us, length us, event | category | flops | bytes accessed | tf_op | source)
XLA Modules:
  0.0 38.2 jit_solution(7535229260602569884)
XLA Ops:
  0.6 36.1 %shard_map.131 = (f32[2,2,32,128]{3,2,1,0:T(8,128)}, f32[2,128]{1,0:T(2,128)}) custom-call(bf16[2,512,2048]{2,1,0:T(8,128)(2,1)} %x_hbm.1, bf16[2048,256]{1,0:T(8,128)(2,1)} %wk_hbm.1, bf16[2048,256]{1,0:T(8,128)(2,1)} %wv_hbm.1, bf16[8,2048]{1,0:T(8,128)(2,1)} %bitcast.7, bf16[8,2048]{1,0:T(8,128)(2,1)} %bitcast.8, f32[1,8]{1,0:T(1,128)} %bitcast.10, ...), custom_call_target="tpu_custom_call" | custom-call | tf_op jit(solution)/shard_map/pallas_call | solution.py:488
  36.7 1.5 %shard_map.132 = (bf16[2,2,32,128]{3,2,1,0:T(8,128)(2,1)}, f32[2,128]{1,0:T(2,128)}) custom-call(f32[2,2,32,128]{3,2,1,0:T(8,128)} %get-tuple-element.6.cache_ref, f32[2,128]{1,0:T(2,128)} %get-tuple-element.7.out_ref), custom_call_target="tpu_custom_call" | custom-call | tf_op jit(solution)/shard_map/pallas_call | solution.py:536

commit v3 on v2

--- a/solution.py
+++ b/solution.py
@@ -191,6 +191,7 @@
     features = part_send.shape[2]
     devices = sp_size * tp_size
     last = sp_size - 1
+    meeting = last // 2
     half = DK // 2
     me = lax.axis_index("sp")
     tp_here = lax.axis_index("tp")
@@ -319,37 +320,42 @@
         def _():
             back_copy(0).wait_recv()
 
-        for s in range(seqs):
-            for h in range(heads):
-                row = s * heads + h
-                query = split(back_in[0, row : row + 1])
-                moved = mm3(query, split(maps[s, h]), NT)
+        @pl.when(me > meeting)
+        def _():
+            moves = []
+            for s in range(seqs):
+                for h in range(heads):
+                    row = s * heads + h
+                    moves.append(mm3(split(back_in[0, row : row + 1]), split(maps[s, h]), NT))
+            for row, moved in enumerate(moves):
                 back_out[0, row : row + 1] = moved[:, :DK]
                 back_out[1, row : row + 1] = back_in[1, row : row + 1] + moved[:, DK:]
-
-        @pl.when(me > 0)
-        def _():
             back_copy(me - 1).start()
 
-        @pl.when(me == 0)
-        def _():
+        @pl.when(me == meeting)
+        def _():
+            reads = []
+            for row in range(pairs):
+                query = split(back_in[0, row : row + 1])
+                reads.append([mm3(query, split(state_out[row, t]), NT) for t in range(2)])
             gates = jax.nn.silu(gate_ref[...].astype(F32))
             norm_send[...] = jnp.zeros_like(norm_send)
             for s in range(seqs):
                 for h in range(heads):
                     row = s * heads + h
-                    readout = back_out[1, row : row + 1]
+                    readout = back_in[1, row : row + 1] + jnp.concatenate(reads[row], axis=1)
                     mean = jnp.mean(readout * readout, axis=1, keepdims=True)
                     scaled = readout * lax.rsqrt(mean + epsilon)
                     gate = gates[s : s + 1, h * DK : (h + 1) * DK]
                     to = h * seqs + s
                     norm_send[to : to + 1] = bf(scaled * gain_ref[...] * gate).astype(F32)
-            for d in range(1, sp_size):
-                norm_copy(d).start()
+            for d in range(sp_size):
+                if d != meeting:
+                    norm_copy(d).start()
             norm_recv[...] = norm_send[...]
 
     def out_step():
-        @pl.when(me > 0)
+        @pl.when(me != meeting)
         def _():
             norm_copy(0).wait_recv()
 
@@ -392,28 +398,17 @@
                                 cols_send[d, p] = state[at : at + columns]
                                 cols_copy(p, d).start()
 
-    middle = pairs // 2
-    late = 2 * me >= sp_size
-
-    @pl.when(late)
+    @pl.when(me > meeting)
     def _():
         back_step()
 
-    state_steps(range(middle))
-
-    @pl.when(jnp.logical_not(late))
+    state_steps(range(pairs))
+
+    @pl.when(me == meeting)
     def _():
         back_step()
 
-    @pl.when(me == last)
-    def _():
-        out_step()
-
-    state_steps(range(middle, pairs))
-
-    @pl.when(me < last)
-    def _():
-        out_step()
+    out_step()
 
     each_other(lambda step, target: part_copy(step, target, target).wait_recv())
 
@@ -441,14 +436,15 @@
             for p in range(pairs):
                 cols_copy(p, d).wait_send()
 
-    @pl.when(me > 0)
+    @pl.when(me > meeting)
     def _():
         back_copy(me - 1).wait_send()
 
-    @pl.when(me == 0)
+    @pl.when(me == meeting)
     def _():
-        for d in range(1, sp_size):
-            norm_copy(d).wait_send()
+        for d in range(sp_size):
+            if d != meeting:
+                norm_copy(d).wait_send()
 
 
 def finish_kernel(cache_ref, out_ref, cache_out, out_out):

time: 38.3 us -> 36 us (0.940)
  Pallas kernels: 37.5 us -> 35.2 us
    pallas_call x1, Pallas kernels: 36.1 us -> 33.7 us  [per_device(): pl.pallas_call(functools.partial(mixer_kernel, sp_size, tp_size), in_spec...]
where the time goes in v3:
time: 36 us; the launch traced here: 35.8 us
  Pallas kernels  35.2 us (98%)
  between operations  0.64 us (2%)
    pallas_call x1, Pallas kernels, per_device(): pl.pallas_call(functools.partial(mixer_kernel, sp_size, tp_size), in_spec...  33.7 us
    pallas_call x1, Pallas kernels, per_device(): pl.pallas_call(finish_kernel, in_specs=[vmem] * 2, out_specs=(vmem, vmem)...  1.47 us

profile of v3, /device:TPU:0, one launch (start us, length us, event | category | flops | bytes accessed | tf_op | source)
XLA Modules:
  0.0 35.8 jit_solution(14843140773752668177)
XLA Ops:
  0.6 33.7 %shard_map.131 = (f32[2,2,32,128]{3,2,1,0:T(8,128)}, f32[2,128]{1,0:T(2,128)}) custom-call(bf16[2,512,2048]{2,1,0:T(8,128)(2,1)} %x_hbm.1, bf16[2048,256]{1,0:T(8,128)(2,1)} %wk_hbm.1, bf16[2048,256]{1,0:T(8,128)(2,1)} %wv_hbm.1, bf16[8,2048]{1,0:T(8,128)(2,1)} %bitcast.7, bf16[8,2048]{1,0:T(8,128)(2,1)} %bitcast.8, f32[1,8]{1,0:T(1,128)} %bitcast.10, ...), custom_call_target="tpu_custom_call" | custom-call | tf_op jit(solution)/shard_map/pallas_call | solution.py:484
  34.4 1.5 %shard_map.132 = (bf16[2,2,32,128]{3,2,1,0:T(8,128)(2,1)}, f32[2,128]{1,0:T(2,128)}) custom-call(f32[2,2,32,128]{3,2,1,0:T(8,128)} %get-tuple-element.6.cache_ref, f32[2,128]{1,0:T(2,128)} %get-tuple-element.7.out_ref), custom_call_target="tpu_custom_call" | custom-call | tf_op jit(solution)/shard_map/pallas_call | solution.py:532

commit v4 on v3

--- a/solution.py
+++ b/solution.py
@@ -174,6 +174,7 @@
     norm_recv,
     part_send,
     part_recv,
+    peer_maps,
     load_sem,
     chain_send_sem,
     chain_recv_sem,
@@ -184,6 +185,8 @@
     norm_recv_sem,
     part_send_sem,
     part_recv_sem,
+    peer_send_sem,
+    peer_recv_sem,
 ):
     seqs, heads = maps.shape[:2]
     pairs = seqs * heads
@@ -193,6 +196,10 @@
     last = sp_size - 1
     meeting = last // 2
     half = DK // 2
+    ends = [last] * pairs
+    if sp_size > 2:
+        for p in range(seqs // 2 * heads, pairs):
+            ends[p] = last - 1
     me = lax.axis_index("sp")
     tp_here = lax.axis_index("tp")
     rank = me * tp_size + tp_here
@@ -261,6 +268,17 @@
             send_sem=norm_send_sem.at[d],
             recv_sem=norm_recv_sem,
             device_id={"sp": d},
+            device_id_type=MESH,
+        )
+
+    def peer_copy(p):
+        s, h = divmod(p, heads)
+        return pltpu.make_async_remote_copy(
+            src_ref=maps.at[s, h],
+            dst_ref=peer_maps.at[s, h],
+            send_sem=peer_send_sem.at[p],
+            recv_sem=peer_recv_sem.at[p],
+            device_id={"sp": last - 1},
             device_id_type=MESH,
         )
 
@@ -372,37 +390,54 @@
         each_other(lambda step, target: part_copy(step, target, rank).start())
         part_recv[rank] = part_send[rank]
 
-    def state_steps(chosen):
-        @pl.when(me > 0)
-        def _():
-            for p in chosen:
-                s, h = divmod(p, heads)
-                linear = split(maps[s, h, :DK])
-                for t in range(2):
-                    offset = maps[s, h, DK + t * half : DK + (t + 1) * half]
-                    chain_copy(p, t, 0).wait_recv()
-                    state = mm3(split(state_in[p, t]), linear) + offset
-                    state_out[p, t] = state
-
-                    @pl.when(me < last)
-                    def _():
-                        chain_copy(p, t, me + 1).start()
-
-                    @pl.when(me == last)
-                    def _():
-                        for d in range(t * half // columns, (t + 1) * half // columns):
-                            at = d * columns - t * half
-                            if d == last:
-                                cols_recv[p] = state[at : at + columns]
-                            else:
-                                cols_send[d, p] = state[at : at + columns]
-                                cols_copy(p, d).start()
+    def scatter(p, t, state):
+        for d in range(t * half // columns, (t + 1) * half // columns):
+            at = d * columns - t * half
+            if d == ends[p]:
+                cols_recv[p] = state[at : at + columns]
+            else:
+                cols_send[d, p] = state[at : at + columns]
+                cols_copy(p, d).start()
+
+    def state_step(p):
+        s, h = divmod(p, heads)
+        linear = split(maps[s, h, :DK])
+        for t in range(2):
+            rows_here = slice(DK + t * half, DK + (t + 1) * half)
+            chain_copy(p, t, 0).wait_recv()
+            state = mm3(split(state_in[p, t]), linear) + maps[s, h, rows_here]
+            state_out[p, t] = state
+
+            @pl.when(me < ends[p])
+            def _():
+                chain_copy(p, t, me + 1).start()
+
+            @pl.when(me == ends[p])
+            def _():
+                if ends[p] == last:
+                    scatter(p, t, state)
+                else:
+                    if t == 0:
+                        peer_copy(p).wait_recv()
+                    ahead = split(peer_maps[s, h, :DK])
+                    scatter(p, t, mm3(split(state), ahead) + peer_maps[s, h, rows_here])
 
     @pl.when(me > meeting)
     def _():
         back_step()
 
-    state_steps(range(pairs))
+    peers = [p for p in range(pairs) if ends[p] < last]
+
+    @pl.when(me == last)
+    def _():
+        for p in peers:
+            peer_copy(p).start()
+
+    for p in range(pairs):
+
+        @pl.when((me > 0) & (me <= ends[p]))
+        def _():
+            state_step(p)
 
     @pl.when(me == meeting)
     def _():
@@ -417,11 +452,15 @@
 
     out_ref[...] = lax.fori_loop(0, devices, add, jnp.zeros(out_ref.shape, F32), unroll=unroll)
 
-    @pl.when(me < last)
-    def _():
-        for p in range(pairs):
+    for p in range(pairs):
+
+        @pl.when(me < ends[p])
+        def _():
             for t in range(2):
                 chain_copy(p, t, me + 1).wait_send()
+
+        @pl.when(me != ends[p])
+        def _():
             cols_copy(p, 0).wait_recv()
 
     for p in range(pairs):
@@ -430,11 +469,18 @@
 
     each_other(lambda step, target: part_copy(step, target, rank).wait_send())
 
+    for p in range(pairs):
+
+        @pl.when(me == ends[p])
+        def _():
+            for d in range(sp_size):
+                if d != ends[p]:
+                    cols_copy(p, d).wait_send()
+
     @pl.when(me == last)
     def _():
-        for d in range(last):
-            for p in range(pairs):
-                cols_copy(p, d).wait_send()
+        for p in peers:
+            peer_copy(p).wait_send()
 
     @pl.when(me > meeting)
     def _():
@@ -501,6 +547,7 @@
             pltpu.VMEM((rows, DK), F32),
             pltpu.VMEM((devices, seqs, features), F32),
             pltpu.VMEM((devices, seqs, features), F32),
+            pltpu.VMEM((seqs, heads, 2 * DK, DK), F32),
             dma((2 + seqs,)),
             dma((pairs, 2)),
             dma((pairs, 2)),
@@ -511,6 +558,8 @@
             dma,
             dma((devices,)),
             dma((devices,)),
+            dma((pairs,)),
+            dma((pairs,)),
         ],
         compiler_params=pltpu.CompilerParams(
             collective_id=0, has_side_effects=True, vmem_limit_bytes=62 * 1024 * 1024

time: 36 us -> 35.1 us (0.975)
  Pallas kernels: 35.2 us -> 34.3 us
    pallas_call x1, Pallas kernels: 33.7 us -> 32.8 us  [per_device(): pl.pallas_call(functools.partial(mixer_kernel, sp_size, tp_size), in_spec...]
where the time goes in v4:
time: 35.1 us; the launch traced here: 34.9 us
  Pallas kernels  34.3 us (98%)
  between operations  0.64 us (2%)
    pallas_call x1, Pallas kernels, per_device(): pl.pallas_call(functools.partial(mixer_kernel, sp_size, tp_size), in_spec...  32.8 us
    pallas_call x1, Pallas kernels, per_device(): pl.pallas_call(finish_kernel, in_specs=[vmem] * 2, out_specs=(vmem, vmem)...  1.47 us

profile of v4, /device:TPU:0, one launch (start us, length us, event | category | flops | bytes accessed | tf_op | source)
XLA Modules:
  0.0 34.9 jit_solution(5147191610759177809)
XLA Ops:
  0.6 32.8 %shard_map.131 = (f32[2,2,32,128]{3,2,1,0:T(8,128)}, f32[2,128]{1,0:T(2,128)}) custom-call(bf16[2,512,2048]{2,1,0:T(8,128)(2,1)} %x_hbm.1, bf16[2048,256]{1,0:T(8,128)(2,1)} %wk_hbm.1, bf16[2048,256]{1,0:T(8,128)(2,1)} %wv_hbm.1, bf16[8,2048]{1,0:T(8,128)(2,1)} %bitcast.7, bf16[8,2048]{1,0:T(8,128)(2,1)} %bitcast.8, f32[1,8]{1,0:T(1,128)} %bitcast.10, ...), custom_call_target="tpu_custom_call" | custom-call | tf_op jit(solution)/shard_map/pallas_call | solution.py:530
  33.4 1.5 %shard_map.132 = (bf16[2,2,32,128]{3,2,1,0:T(8,128)(2,1)}, f32[2,128]{1,0:T(2,128)}) custom-call(f32[2,2,32,128]{3,2,1,0:T(8,128)} %get-tuple-element.6.cache_ref, f32[2,128]{1,0:T(2,128)} %get-tuple-element.7.out_ref), custom_call_target="tpu_custom_call" | custom-call | tf_op jit(solution)/shard_map/pallas_call | solution.py:581
